TPU v7x, 256 devices: a whole 4x4x8 slice. The times are simulated.
256 devices in a mesh: sp: 32 (over z, y), dp: 8 (over x, core).
Axes of the slice: x: 4, y: 4, z: 8, core: 2. Of those that a mesh axis runs over, the one named last changes fastest.
Arguments:
- queries: bfloat16 [32768, 6144], P(('dp', 'sp')), may hold values from -360 to 360
- latent: bfloat16 [32768, 1024], P(('dp', 'sp')), may hold values from -6 to 6
- rope_key: bfloat16 [32768, 64], P(('dp', 'sp')), may hold values from -6 to 6
- latent_gain: float32 [1024], replicated, may hold values from 0.1 to 1.9
- kv_weight: bfloat16 [1024, 8192], P(None, 'dp'), may hold values from -0.1875 to 0.1875
- gate: bfloat16 [32768, 4096], P(('dp', 'sp')), may hold values from -6 to 6
- out_gain: float32 [4096], replicated, may hold values from 0.1 to 1.9
Outputs:
- attended: bfloat16 [32768, 4096], P(('dp', 'sp'))
All inputs are finite; a program needn't handle non-finite values.
Results may differ from a plain program's by a relative error of at most 0.007.
Values may be sent and summed in bfloat16 or wider, within the bound.
A program may use at most 128 MiB of HBM per device.

v0:
```python
import jax
import jax.numpy as jnp
from jax import lax
from jax.sharding import PartitionSpec as P

HEADS = 32
NOPE = 128
ROPE = 64
VDIM = 128


EPS = 1e-06
THETA = 10000.0


def in_order(blocks, dim):
    blocks = jnp.moveaxis(blocks, 0, dim)
    shape = blocks.shape
    return blocks.reshape(*shape[:dim], shape[dim] * shape[dim + 1], *shape[dim + 2 :])


def copy_for_each(value, axis):
    length = lax.axis_size(axis)
    return lax.all_to_all(
        jnp.broadcast_to(value[None], (length, *value.shape)), axis, 0, 0, tiled=True
    )


def gathered_copies(value, axis, dim):
    return in_order(copy_for_each(value, axis), dim)


def rotary(values, position):
    half_width = values.shape[-1] // 2
    inverse = THETA ** (-jnp.arange(half_width, dtype=jnp.float32) / half_width)
    angles = position.astype(jnp.float32)[:, None] * inverse[None, :]
    if values.ndim == 3:
        angles = angles[:, None, :]
    cosine = jnp.cos(angles)
    sine_part = jnp.sin(angles)
    front_half = values[..., :half_width].astype(jnp.float32)
    back_half = values[..., half_width:].astype(jnp.float32)
    turned = jnp.concatenate(
        [front_half * cosine - back_half * sine_part, back_half * cosine + front_half * sine_part],
        axis=-1,
    )
    return turned.astype(jnp.bfloat16)


def attend(query_block, keys_plain, keys_rotated, values):
    scores = jnp.einsum(
        "qhd,khd->hqk", query_block[..., :NOPE], keys_plain, preferred_element_type=jnp.float32
    )
    scores = scores + jnp.einsum(
        "qhr,kr->hqk", query_block[..., NOPE:], keys_rotated, preferred_element_type=jnp.float32
    )
    scores = scores * (NOPE + ROPE) ** (-0.5)
    row_max = jnp.max(scores, axis=-1, keepdims=True)
    raised = jnp.exp(scores - row_max)
    weights = (raised / jnp.sum(raised, axis=-1, keepdims=True)).astype(jnp.bfloat16)
    result = jnp.einsum("hqk,khd->qhd", weights, values, preferred_element_type=jnp.float32)
    return result.astype(jnp.bfloat16)


def per_device(queries, latent, rope_key, latent_gain, kv_weight, gate, out_gain):
    own_tokens = queries.shape[0]
    groups = lax.axis_size("sp")
    seq_len = own_tokens * groups
    offset = lax.axis_index("sp") * own_tokens
    position = offset + jnp.arange(own_tokens, dtype=jnp.int32)
    widened = latent.astype(jnp.float32)
    normed = (
        widened * lax.rsqrt(jnp.mean(widened * widened, axis=-1, keepdims=True) + EPS) * latent_gain
    ).astype(jnp.bfloat16)
    keyval = jnp.dot(
        normed,
        lax.all_gather(kv_weight, "dp", axis=1, tiled=True),
        preferred_element_type=jnp.float32,
    ).astype(jnp.bfloat16)
    head_queries = queries.reshape(own_tokens, HEADS, NOPE + ROPE)
    head_queries = jnp.concatenate(
        [head_queries[..., :NOPE], rotary(head_queries[..., NOPE:], position)], axis=-1
    )
    head_queries = head_queries.reshape(own_tokens, HEADS * (NOPE + ROPE))
    rotated_all = gathered_copies(rotary(rope_key, position), "sp", 0)
    query_all, kv_all = (
        lax.all_to_all(head_queries, "sp", split_axis=1, concat_axis=0, tiled=True),
        lax.all_to_all(keyval, "sp", split_axis=1, concat_axis=0, tiled=True),
    )
    local_heads = HEADS // groups
    rows_all = query_all.shape[0]
    seq_count = rows_all // seq_len
    block_rows = min(512, seq_len)
    block_count = seq_len // block_rows

    def one_sequence(operands):
        query_seq, kv_seq, rope_seq = operands
        keys_plain = kv_seq[..., :NOPE]
        values = kv_seq[..., NOPE:]
        blocks = query_seq.reshape(block_count, block_rows, local_heads, NOPE + ROPE)
        result = lax.map(
            lambda piece_rows: attend(piece_rows, keys_plain, rope_seq, values), blocks
        )
        return result.reshape(seq_len, local_heads * VDIM)

    heads_out = lax.map(
        one_sequence,
        (
            query_all.reshape(seq_count, seq_len, local_heads, NOPE + ROPE),
            kv_all.reshape(seq_count, seq_len, local_heads, NOPE + VDIM),
            rotated_all.reshape(seq_count, seq_len, ROPE),
        ),
    )
    heads_out = heads_out.reshape(rows_all, local_heads * VDIM)
    token_rows = lax.all_to_all(heads_out, "sp", split_axis=0, concat_axis=1, tiled=True)
    gated_rows = token_rows.astype(jnp.float32) * jax.nn.silu(gate.astype(jnp.float32))
    scale_rows = lax.rsqrt(jnp.mean(gated_rows * gated_rows, axis=-1, keepdims=True) + EPS)
    return (gated_rows * scale_rows * out_gain).astype(jnp.bfloat16)


def solution(mesh):
    return jax.shard_map(
        per_device,
        mesh=mesh,
        in_specs=(
            P(("dp", "sp"), None),
            P(("dp", "sp"), None),
            P(("dp", "sp"), None),
            P(),
            P(None, "dp"),
            P(("dp", "sp"), None),
            P(),
        ),
        out_specs=P(("dp", "sp"), None),
        check_vma=False,
    )
```

profile of v0, /device:TPU:1, one launch (start us, length us, event | category | flops | bytes accessed | tf_op | source)
XLA Modules:
  0.0 276.5 jit_solution(5976931859334378445)
XLA Ops:
  8.4 12.0 %all-to-all-start.2 = ((bf16[32,128,64]{1,2,0:T(8,128)(2,1)}), bf16[32,128,64]{1,2,0:T(8,128)(2,1)S(1)}, u32[]{:S(2)}, u32[]{:S(2)}) async-start(bf16[32,128,64]{1,2,0:T(8,128)(2,1)} %broadcast_in_dim.7), calls=%async_computation.2 | async-start | bytes 1048576 | tf_op jit(solution)/shard_map/all_to_all | solution.py:24
  20.4 1.9 copy.26
  23.9 12.8 %all-to-all-done.2 = bf16[32,128,64]{1,2,0:T(8,128)(2,1)S(1)} async-done(((bf16[32,128,64]{1,2,0:T(8,128)(2,1)}), bf16[32,128,64]{1,2,0:T(8,128)(2,1)S(1)}, u32[]{:S(2)}, u32[]{:S(2)}) %all-to-all-start.2) | async-done | bytes 524320 | tf_op jit(solution)/shard_map/all_to_all | solution.py:24
  36.7 5.3 %all-to-all-start = ((bf16[128,32,192]{0,2,1:T(8,128)(2,1)}), bf16[128,32,192]{0,2,1:T(8,128)(2,1)S(1)}, u32[]{:S(2)}, u32[]{:S(2)}) async-start(bf16[128,32,192]{0,2,1:T(8,128)(2,1)} %pad_maximum_fusion), calls=%async_computation | async-start | bytes 3145728 | tf_op jit(solution)/shard_map/all_to_all | solution.py:87
  42.1 58.7 %all-gather.2.cloned.1.call-done = bf16[1024,8192]{1,0:T(8,128)(2,1)} async-done(((bf16[1024,1024]{1,0:T(8,128)(2,1)}), bf16[1024,8192]{1,0:T(8,128)(2,1)}) %all-gather.2.cloned.1.call-update) | async-done | bytes 16777232 | tf_op jit(solution)/shard_map/all_gather | solution.py:77
  100.8 8.2 %convolution_convert_fusion = bf16[128,8192]{1,0:T(8,128)(2,1)S(1)} fusion(bf16[1024,8192]{1,0:T(8,128)(2,1)} %all-gather.2.cloned.1.call-done, bf16[128,1024]{1,0:T(8,128)(2,1)S(1)} %copy-done.3, f32[1024]{0:T(1024)S(1)} %copy-done.8, f32[128]{0:T(128)S(1)} %add_rsqrt_fusion.1), kind=kOutput, calls=%fused_computation.16 | convolution fusion | flops 2149056512 | bytes 19141120 | tf_op jit(solution)/shard_map/dot_general | solution.py:75
  109.0 1.6 copy.39
  111.8 9.8 %all-to-all-start.1 = ((bf16[128,32,256]{2,0,1:T(8,128)(2,1)}), bf16[128,32,256]{2,0,1:T(8,128)(2,1)S(1)}, u32[]{:S(2)}, u32[]{:S(2)}) async-start(bf16[128,32,256]{2,0,1:T(8,128)(2,1)} %bitcast.86), calls=%async_computation.1 | async-start | bytes 4194304 | tf_op jit(solution)/shard_map/all_to_all | solution.py:88
  123.1 3.6 %copy.27 = bf16[32,128,192]{1,0,2:T(8,128)(2,1)} copy(bf16[32,128,192]{1,2,0:T(8,128)(2,1)} %bitcast.88) | data formatting | bytes 3145728 | tf_op jit(solution)/shard_map/all_to_all | solution.py:87
  126.7 3.7 %reshape.157 = bf16[8,512,1,192]{1,0,3,2:T(8,128)(2,1)} reshape(bf16[32,128,192]{1,0,2:T(8,128)(2,1)} %copy.27) | data formatting | bytes 3145728 | tf_op jit(solution)/shard_map/while/body/eval_jaxpr/reshape | solution.py:100
  130.4 3.1 %copy.30 = bf16[8,512,1,192]{1,3,2,0:T(8,128)(2,1)} copy(bf16[8,512,1,192]{1,0,3,2:T(8,128)(2,1)} %reshape.157) | data formatting | bytes 3145728 | tf_op jit(solution)/shard_map/while/body/eval_jaxpr/while | solution.py:101
  133.5 36.5 %all-to-all-done.1 = bf16[128,32,256]{2,0,1:T(8,128)(2,1)S(1)} async-done(((bf16[128,32,256]{2,0,1:T(8,128)(2,1)}), bf16[128,32,256]{2,0,1:T(8,128)(2,1)S(1)}, u32[]{:S(2)}, u32[]{:S(2)}) %all-to-all-start.1) | async-done | bytes 2097184 | tf_op jit(solution)/shard_map/all_to_all | solution.py:88
  171.3 2.7 fusion.35
  174.0 57.8 %while.17 = (s32[]{:T(128)}, bf16[8,512,1,128]{3,1,2,0:T(8,128)(2,1)S(1)}, bf16[8,512,1,192]{1,3,2,0:T(8,128)(2,1)}, bf16[4096,1,128]{2,0,1:T(8,128)(2,1)S(1)}, ...) while((s32[]{:T(128)}, bf16[8,512,1,128]{3,1,2,0:T(8,128)(2,1)S(1)}, ...), condition=%wide.region_4.5_spmd, body=%wide.region_1.4_spmd.sunk | while | flops 1359019008 | bytes 50014328 | solution.py:101
  179.0 2.2 fusion.53
  186.2 2.2 fusion.53
  193.4 2.2 fusion.53
  200.6 2.2 fusion.53
  207.9 2.2 fusion.53
  215.1 2.2 fusion.53
  222.3 2.2 fusion.53
  229.5 2.2 fusion.53
  232.8 7.0 %all-to-all-start.3 = ((bf16[32,128,128]{2,1,0:T(8,128)(2,1)}), bf16[32,128,128]{2,1,0:T(8,128)(2,1)S(1)}, u32[]{:S(2)}, u32[]{:S(2)}) async-start(bf16[32,128,128]{2,1,0:T(8,128)(2,1)} %bitcast.91), calls=%async_computation.3 | async-start | bytes 2097152 | tf_op jit(solution)/shard_map/all_to_all | solution.py:115
  240.5 25.6 %all-to-all-done.3 = bf16[32,128,128]{2,1,0:T(8,128)(2,1)S(1)} async-done(((bf16[32,128,128]{2,1,0:T(8,128)(2,1)}), bf16[32,128,128]{2,1,0:T(8,128)(2,1)S(1)}, u32[]{:S(2)}, u32[]{:S(2)}) %all-to-all-start.3) | async-done | bytes 1048608 | tf_op jit(solution)/shard_map/all_to_all | solution.py:115
  (89 shorter events, 52.3 us)
Async XLA Ops:
  6.5 0.8 copy-start.10
  6.5 94.3 %all-gather.2.cloned.1.call-start = ((), (), s32[]{:S(2)}) async-start(), calls=%async_computation.4 | async-start | bytes 18874368 | tf_op jit(solution)/shard_map/all_gather | solution.py:77
  8.4 28.3 %all-to-all-start.2 = ((bf16[32,128,64]{1,2,0:T(8,128)(2,1)}), bf16[32,128,64]{1,2,0:T(8,128)(2,1)S(1)}, u32[]{:S(2)}, u32[]{:S(2)}) async-start(bf16[32,128,64]{1,2,0:T(8,128)(2,1)} %broadcast_in_dim.7), calls=%async_computation.2 | async-start | bytes 1048576 | tf_op jit(solution)/shard_map/all_to_all | solution.py:24
  23.9 18.0 %copy-start.3 = (bf16[128,1024]{1,0:T(8,128)(2,1)S(1)}, bf16[128,1024]{1,0:T(8,128)(2,1)}, u32[]{:S(2)}) copy-start(bf16[128,1024]{1,0:T(8,128)(2,1)} %param.10) | copy-start | bytes 786436
  23.9 76.9 %copy-start.8 = (f32[1024]{0:T(1024)S(1)}, f32[1024]{0:T(1024)}, u32[]{:S(2)}) copy-start(f32[1024]{0:T(1024)} %param.12) | copy-start | bytes 12292
  36.7 72.3 %copy-start.2 = (bf16[32,128,64]{1,2,0:T(8,128)(2,1)}, bf16[32,128,64]{1,2,0:T(8,128)(2,1)S(1)}, u32[]{:S(2)}) copy-start(bf16[32,128,64]{1,2,0:T(8,128)(2,1)S(1)} %all-to-all-done.2) | copy-start | bytes 1572868
  36.7 73.9 %all-to-all-start = ((bf16[128,32,192]{0,2,1:T(8,128)(2,1)}), bf16[128,32,192]{0,2,1:T(8,128)(2,1)S(1)}, u32[]{:S(2)}, u32[]{:S(2)}) async-start(bf16[128,32,192]{0,2,1:T(8,128)(2,1)} %pad_maximum_fusion), calls=%async_computation | async-start | bytes 3145728 | tf_op jit(solution)/shard_map/all_to_all | solution.py:87
  110.6 1.2 copy-start.1
  111.8 58.1 %all-to-all-start.1 = ((bf16[128,32,256]{2,0,1:T(8,128)(2,1)}), bf16[128,32,256]{2,0,1:T(8,128)(2,1)S(1)}, u32[]{:S(2)}, u32[]{:S(2)}) async-start(bf16[128,32,256]{2,0,1:T(8,128)(2,1)} %bitcast.86), calls=%async_computation.1 | async-start | bytes 4194304 | tf_op jit(solution)/shard_map/all_to_all | solution.py:88
  169.9 1.3 copy-start
  171.3 2.7 copy-start.5
  177.7 1.3 copy-start.7
  184.9 1.3 copy-start.7
  192.1 1.3 copy-start.7
  199.3 1.3 copy-start.7
  206.6 1.3 copy-start.7
  213.8 1.3 copy-start.7
  221.0 1.3 copy-start.7
  228.2 1.3 copy-start.7
  231.8 1.0 copy-start.6
  231.8 8.0 %copy-start.4 = (bf16[128,4096]{1,0:T(8,128)(2,1)S(1)}, bf16[128,4096]{1,0:T(8,128)(2,1)}, u32[]{:S(2)}) copy-start(bf16[128,4096]{1,0:T(8,128)(2,1)} %param.14) | copy-start | bytes 3145732
  232.8 33.3 %all-to-all-start.3 = ((bf16[32,128,128]{2,1,0:T(8,128)(2,1)}), bf16[32,128,128]{2,1,0:T(8,128)(2,1)S(1)}, u32[]{:S(2)}, u32[]{:S(2)}) async-start(bf16[32,128,128]{2,1,0:T(8,128)(2,1)} %bitcast.91), calls=%async_computation.3 | async-start | bytes 2097152 | tf_op jit(solution)/shard_map/all_to_all | solution.py:115
  240.5 27.0 %copy-start.9 = (f32[4096]{0:T(1024)S(1)}, f32[4096]{0:T(1024)}, u32[]{:S(2)}) copy-start(f32[4096]{0:T(1024)} %param.15) | copy-start | bytes 49156
Sparse Core Ops, SparseCore 0:
  9.2 91.6 all-gather.1
where the time goes:
time: 279 us; the launch traced here: 276 us
  waiting for transfers between devices  134 us (48%)
  matrix products  47.9 us (17%)
  starting transfers between devices  34 us (12%)
  local copies, waits for them, and re-layouts  32.8 us (12%)
  other arithmetic  13.6 us (5%)
  between operations  13.6 us (5%)
    all_gather x1, waiting for transfers between devices, per_device(): lax.all_gather(kv_weight, 'dp', axis=1, tiled=True)  58.7 us
    all_to_all x1, waiting for transfers between devices, per_device(): lax.all_to_all(keyval, 'sp', split_axis=1, concat_axis=0, tiled=True)  36.5 us
    all_to_all x1, waiting for transfers between devices, per_device(): lax.all_to_all(heads_out, 'sp', split_axis=0, concat_axis=1, tiled=True)  25.6 us
    dot_general x8, matrix products, attend(): jnp.einsum('hqk,khd->qhd', weights, values, preferred_element_type=jnp.fl...  18 us
    all_to_all x1, waiting for transfers between devices, copy_for_each(): lax.all_to_all(jnp.broadcast_to(value[None], (length, *value.shape)), axi...  12.8 us
    all_to_all x1, starting transfers between devices, copy_for_each(): lax.all_to_all(jnp.broadcast_to(value[None], (length, *value.shape)), axi...  12 us
    dot_general x8, matrix products, attend(): jnp.einsum('qhr,kr->hqk', query_block[..., NOPE:], keys_rotated, preferre...  11.4 us
    dot_general x8, matrix products, attend(): jnp.einsum('qhd,khd->hqk', query_block[..., :NOPE], keys_plain, preferred...  10.3 us
  transfers between devices with their start and end apart: 5, of which 4 were waited for; matrix products, arithmetic and copies ran while one was open for 10% of the time, Pallas kernels for 0%

commit v1 on v0

v1 whole, which is shorter than its diff:
```python
import functools

import jax
import jax.numpy as jnp
from jax import lax
from jax.experimental import pallas as pl
from jax.experimental.pallas import tpu as pltpu
from jax.sharding import PartitionSpec as P

HEADS = 32
NOPE = 128
ROPE = 64
VDIM = 128
RANK = 1024
EPS = 1e-06
THETA = 10000.0
LOG2E = 1.4426950408889634
SCALE = (NOPE + ROPE) ** (-0.5) * LOG2E
NX, NY, NZ = 4, 4, 8
WIDE = RANK + 128
NT = (((1,), (1,)), ((), ()))
BF16 = jnp.bfloat16
F32 = jnp.float32


def rotary(values, position):
    half_width = values.shape[-1] // 2
    inverse = THETA ** (-jnp.arange(half_width, dtype=F32) / half_width)
    angles = position.astype(F32)[:, None] * inverse[None, :]
    if values.ndim == 3:
        angles = angles[:, None, :]
    cosine = jnp.cos(angles)
    sine_part = jnp.sin(angles)
    front_half = values[..., :half_width].astype(F32)
    back_half = values[..., half_width:].astype(F32)
    turned = jnp.concatenate(
        [front_half * cosine - back_half * sine_part, back_half * cosine + front_half * sine_part],
        axis=-1,
    )
    return turned.astype(BF16)


def body(
    lat_in, q_in, w_in, gate, gain, out,
    lat, q, w, k_s, vt_s, m_s, l_s, acc_s, o_buf, o_ret, gated,
    y_send, y_recv, ring_send, ring_recv, pair_send, pair_recv,
    q_send, q_recv, w_send, w_recv, o_send, o_recv,
):
    sp, dp = lax.axis_index("sp"), lax.axis_index("dp")
    z, y = sp // NY, sp % NY
    x, core = dp // 2, dp % 2
    seq, role = y // 2, y % 2
    native = core == role
    zp, zm = (z + 1) % NZ, (z + NZ - 1) % NZ
    xp, xm = (x + 1) % NX, (x + NX - 1) % NX

    def dev(x_, core_, y_, z_):
        return {"sp": z_ * NY + y_, "dp": x_ * 2 + core_}

    def remote(src, dst, send, recv, to):
        return pltpu.make_async_remote_copy(
            src_ref=src, dst_ref=dst, send_sem=send, recv_sem=recv,
            device_id=to, device_id_type=pl.DeviceIdType.MESH,
        )

    partner = dev(x, 1 - core, y, z)
    up, down = dev(x, core, y, zp), dev(x, core, y, zm)

    def pair_of(core_, role_, t):
        is_native = core_ == role_
        slot = jnp.where(is_native, t // 2, t % 2)
        half = jnp.where(is_native, t % 2, t // 2)
        off = jnp.where(is_native, 2 * slot, 2 * slot + 1)
        return (2 * ((x + off) % NX) + role_) * 2 + half

    barrier = pltpu.get_barrier_semaphore()
    for yy in range(NY):
        for cc in range(2):
            @pl.when(jnp.logical_or(yy != y, cc != core))
            def _():
                pl.semaphore_signal(barrier, inc=1, device_id=dev(x, cc, yy, z), device_id_type=pl.DeviceIdType.MESH)
    for to in (up, down, dev(xp, 0, y, z), dev(xp, 1, y, z), dev(xm, 0, y, z), dev(xm, 1, y, z)):
        pl.semaphore_signal(barrier, inc=1, device_id=to, device_id_type=pl.DeviceIdType.MESH)
    pl.semaphore_wait(barrier, 13)

    dests = [(rr, kk) for rr in range(2) for kk in range(2)]

    def is_self(rr, kk):
        return jnp.logical_and(y == 2 * core + rr, kk == core)

    def lat_copy(rr, kk):
        return remote(
            lat_in.at[kk], lat.at[z, kk, y], y_send.at[rr, kk], y_recv.at[y],
            dev(x, kk, 2 * core + rr, z),
        )

    def q_copy(rr, kk, t):
        return remote(
            q_in.at[pair_of(kk, rr, t)], q.at[t, y], q_send.at[t, rr, kk], q_recv.at[t, y],
            dev(x, kk, 2 * core + rr, z),
        )

    for rr, kk in dests:
        @pl.when(is_self(rr, kk))
        def _():
            pltpu.make_async_copy(lat_in.at[kk], lat.at[z, kk, y], y_recv.at[y]).start()

        @pl.when(jnp.logical_not(is_self(rr, kk)))
        def _():
            lat_copy(rr, kk).start()

    def w_direct(half, plus):
        to = dev(xp if plus else xm, 1 - role, y, z)
        return remote(
            w_in.at[half], w.at[2 * half + plus], w_send.at[half, plus], w_recv.at[2 * half + plus], to
        )

    def w_relay(half):
        t_here = 1 if half == 0 else 2
        to = dev(xp if half == 0 else xm, role, y, z)
        return remote(
            w.at[t_here], w.at[2 + half], w_send.at[half, 0], w_recv.at[2 + half], to
        )

    @pl.when(native)
    def _():
        for half in range(2):
            pltpu.make_async_copy(w_in.at[half], w.at[half], w_recv.at[half]).start()
        for half in range(2):
            for plus in range(2):
                w_direct(half, plus).start()

    for t in range(4):
        for rr, kk in dests:
            @pl.when(is_self(rr, kk))
            def _():
                pltpu.make_async_copy(
                    q_in.at[pair_of(kk, rr, t)], q.at[t, y], q_recv.at[t, y]
                ).start()

            @pl.when(jnp.logical_not(is_self(rr, kk)))
            def _():
                q_copy(rr, kk, t).start()

    def cut(ref, direction, step):
        return ref.at[pl.ds(2 * direction, 2)] if step == 4 else ref

    def block_of(direction, step):
        return (z + NZ - step) % NZ if direction == 0 else (z + step) % NZ

    def ring(direction, step):
        block = cut(lat.at[block_of(direction, step - 1), core], direction, step)
        return remote(
            block, block, ring_send.at[direction, step - 1], ring_recv.at[direction, step - 1],
            up if direction == 0 else down,
        )

    def ring_arrival(direction, step):
        block = cut(lat.at[block_of(direction, step), core], direction, step)
        return remote(
            block, block, ring_send.at[direction, step - 1], ring_recv.at[direction, step - 1],
            up if direction == 0 else down,
        )

    def to_partner(direction, step):
        block = cut(lat.at[block_of(direction, step), core], direction, step)
        return remote(
            block, block, pair_send.at[direction, step], pair_recv.at[direction, step], partner
        )

    def from_partner(direction, step):
        block = cut(lat.at[block_of(direction, step), 1 - core], direction, step)
        return remote(
            block, block, pair_send.at[direction, step], pair_recv.at[direction, step], partner
        )

    for yy in range(NY):
        remote(lat_in.at[0], lat.at[z, core, yy], y_send.at[0, 0], y_recv.at[yy], partner).wait_recv()
    ring(0, 1).start()
    ring(1, 1).start()
    to_partner(0, 0).start()

    def advance(step):
        for direction in range(2):
            ring_arrival(direction, step).wait_recv()
            if step < 4:
                ring(direction, step + 1).start()
            to_partner(direction, step).start()
        for direction in range(2):
            from_partner(direction, step).wait_recv()

    def w_arrival(t):
        return remote(w_in.at[0], w.at[t], w_send.at[0, 0], w_recv.at[t], partner)

    m_s[...] = jnp.full_like(m_s, -jnp.inf)
    l_s[...] = jnp.zeros_like(l_s)
    acc_s[...] = jnp.zeros_like(acc_s)
    lane = lax.broadcasted_iota(jnp.int32, (1, 128), 1)

    def unit(t, za, zb):
        for i, zz in enumerate((za, zb)):
            lz = lat[zz].reshape(512, WIDE)[:, :RANK]
            keys = lax.dot_general(lz, w[t, :256], NT, preferred_element_type=F32)
            k_s[i * 512:(i + 1) * 512, :] = keys.astype(BF16)
            vals = lax.dot_general(w[t, 256:], lz, NT, preferred_element_type=F32)
            vt_s[:, i * 512:(i + 1) * 512] = vals.astype(BF16)
        turned = jnp.concatenate(
            [lat[zz].reshape(512, WIDE)[:, RANK:] for zz in (za, zb)], axis=0
        )
        for hh in range(2):
            mask = lane < 64 if hh == 0 else lane >= 64
            key = jnp.concatenate(
                [k_s[:, hh * 128:(hh + 1) * 128], jnp.where(mask, turned, jnp.zeros_like(turned))], axis=1
            )
            query = jnp.concatenate(
                [
                    jnp.concatenate([q[t, yy, hh], q[t, yy, 2]], axis=1)
                    for yy in range(NY)
                ],
                axis=0,
            )
            s = lax.dot_general(key, query, NT, preferred_element_type=F32)
            m_old = m_s[t, hh]
            m_new = jnp.maximum(m_old, jnp.max(s, axis=0, keepdims=True) * SCALE)
            p = jnp.exp2(s * SCALE - m_new)
            shrink = jnp.exp2(m_old - m_new)
            l_s[t, hh] = l_s[t, hh] * shrink + jnp.sum(p, axis=0, keepdims=True)
            m_s[t, hh] = m_new
            acc_s[t, hh] = acc_s[t, hh] * shrink + jnp.dot(
                vt_s[hh * 128:(hh + 1) * 128, :], p.astype(BF16), preferred_element_type=F32
            )

    def o_copy(t, yy):
        return remote(
            o_buf.at[t, yy], o_ret.at[pair_of(core, role, t)], o_send.at[t, yy],
            o_recv.at[pair_of(core, role, t)], dev(x, seq, yy, z),
        )

    def o_self(yy):
        return jnp.logical_and(yy == y, seq == core)

    @pl.when(jnp.logical_not(native))
    def _():
        w_arrival(1).wait_recv()
        w_relay(0).start()

    from_partner(0, 0).wait_recv()

    @pl.loop(0, 4)
    def _(step):
        for j in range(4):
            @pl.when(step == j)
            def _():
                advance(j + 1)
        za = jnp.where(step == 3, z, (z + NZ - 1 - step) % NZ)
        zb = (z + 1 + step) % NZ

        @pl.loop(0, 4)
        def _(t):
            @pl.when(step == 0)
            def _():
                @pl.when(jnp.logical_or(native, t != 1))
                def _():
                    w_arrival(t).wait_recv()

                @pl.when(jnp.logical_and(jnp.logical_not(native), t == 2))
                def _():
                    w_relay(1).start()

                for yy in range(NY):
                    remote(q_in.at[0], q.at[t, yy], q_send.at[0, 0, 0], q_recv.at[t, yy], partner).wait_recv()

            unit(t, za, zb)

            @pl.when(step == 3)
            def _():
                for hh in range(2):
                    r = acc_s[t, hh] / l_s[t, hh]
                    for yy in range(NY):
                        piece = r[:, yy * 128:(yy + 1) * 128].T.astype(BF16)
                        o_buf[t, yy, hh] = piece

                        @pl.when(o_self(yy))
                        def _():
                            o_ret[pair_of(core, role, t), hh] = piece
                for yy in range(NY):
                    @pl.when(jnp.logical_not(o_self(yy)))
                    def _():
                        o_copy(t, yy).start()

    total = jnp.zeros((128, 128), F32)
    for t in range(4):
        for rr, kk in dests:
            g = pair_of(kk, rr, t)

            @pl.when(jnp.logical_not(is_self(rr, kk)))
            def _():
                remote(
                    o_buf.at[0, 0], o_ret.at[g], o_send.at[0, 0], o_recv.at[g], partner
                ).wait_recv()
    for h in range(HEADS):
        v = gate[:, h * 128:(h + 1) * 128].astype(F32)
        piece = o_ret[h // 2, h % 2].astype(F32) * (v / (1.0 + jnp.exp(-v)))
        gated[:, h * 128:(h + 1) * 128] = piece
        total = total + piece * piece
    mean = jnp.sum(total, axis=1, keepdims=True) / (HEADS * VDIM)
    scale = lax.rsqrt(mean + EPS)
    for h in range(HEADS):
        cols = slice(h * 128, (h + 1) * 128)
        out[:, cols] = (gated[:, cols] * scale * gain[:, cols]).astype(BF16)

    for rr, kk in dests:
        @pl.when(jnp.logical_not(is_self(rr, kk)))
        def _():
            lat_copy(rr, kk).wait_send()
            for t in range(4):
                q_copy(rr, kk, t).wait_send()

    @pl.when(native)
    def _():
        for half in range(2):
            for plus in range(2):
                w_direct(half, plus).wait_send()

    @pl.when(jnp.logical_not(native))
    def _():
        w_relay(0).wait_send()
        w_relay(1).wait_send()

    to_partner(0, 0).wait_send()
    for direction in range(2):
        for step in range(1, 5):
            ring(direction, step).wait_send()
            to_partner(direction, step).wait_send()
    for t in range(4):
        for yy in range(NY):
            @pl.when(jnp.logical_not(o_self(yy)))
            def _():
                o_copy(t, yy).wait_send()


def per_device(queries, latent, rope_key, latent_gain, kv_weight, gate, out_gain):
    own = queries.shape[0]
    position = lax.axis_index("sp") * own + jnp.arange(own, dtype=jnp.int32)
    widened = latent.astype(F32)
    normed = (
        widened * lax.rsqrt(jnp.mean(widened * widened, axis=-1, keepdims=True) + EPS) * latent_gain
    ).astype(BF16)
    turned_key = rotary(rope_key, position)
    lat_in = jnp.concatenate([normed, turned_key, turned_key], axis=1).reshape(2, 64, WIDE)
    heads = queries.reshape(own, HEADS, NOPE + ROPE)
    turned = rotary(heads[..., NOPE:], position).reshape(own, HEADS // 2, 1, 128)
    plain = heads[..., :NOPE].reshape(own, HEADS // 2, 2, 128)
    q_in = jnp.concatenate([plain, turned], axis=2).transpose(1, 2, 0, 3)
    w_in = kv_weight.reshape(RANK, 2, 2, 2, 128).transpose(1, 3, 2, 4, 0).reshape(2, 512, RANK)
    any_spec = pl.BlockSpec(memory_space=pl.ANY)
    vmem_spec = pl.BlockSpec(memory_space=pltpu.VMEM)
    dma = pltpu.SemaphoreType.DMA
    return pl.pallas_call(
        body,
        out_shape=jax.ShapeDtypeStruct((own, HEADS * VDIM), BF16),
        in_specs=[any_spec, any_spec, any_spec, vmem_spec, vmem_spec],
        out_specs=vmem_spec,
        scratch_shapes=[
            pltpu.VMEM((NZ, 2, NY, 64, WIDE), BF16),
            pltpu.VMEM((4, NY, 3, 128, 128), BF16),
            pltpu.VMEM((4, 512, RANK), BF16),
            pltpu.VMEM((1024, 256), BF16),
            pltpu.VMEM((256, 1024), BF16),
            pltpu.VMEM((4, 2, 1, 512), F32),
            pltpu.VMEM((4, 2, 1, 512), F32),
            pltpu.VMEM((4, 2, 128, 512), F32),
            pltpu.VMEM((4, NY, 2, 128, 128), BF16),
            pltpu.VMEM((16, 2, 128, 128), BF16),
            pltpu.VMEM((own, HEADS * VDIM), F32),
            dma((2, 2)), dma((NY,)), dma((2, 4)), dma((2, 4)), dma((2, 5)), dma((2, 5)),
            dma((4, 2, 2)), dma((4, NY)), dma((2, 2)), dma((4,)), dma((4, NY)), dma((16,)),
        ],
        compiler_params=pltpu.CompilerParams(
            collective_id=0, has_side_effects=True, vmem_limit_bytes=60 * 2**20
        ),
        cost_estimate=pl.CostEstimate(flops=30 * 10**9, bytes_accessed=10**7, transcendentals=0),
        name="latent_attention",
    )(lat_in, q_in, w_in, gate, out_gain.reshape(1, -1))


def solution(mesh):
    return jax.shard_map(
        per_device,
        mesh=mesh,
        in_specs=(
            P(("dp", "sp"), None),
            P(("dp", "sp"), None),
            P(("dp", "sp"), None),
            P(),
            P(None, "dp"),
            P(("dp", "sp"), None),
            P(),
        ),
        out_specs=P(("dp", "sp"), None),
        check_vma=False,
    )
```

time: 279 us -> 132 us (0.47)
  waiting for transfers between devices: 134 us -> 0 us
  Pallas kernels: 0 us -> 114 us
  matrix products: 47.9 us -> 0 us
  starting transfers between devices: 34 us -> 0 us
  local copies, waits for them, and re-layouts: 32.8 us -> 13.2 us
  between operations: 13.6 us -> 0.08 us
  other arithmetic: 13.6 us -> 4.72 us
    pallas_call x0 -> x1, Pallas kernels: none -> 114 us  [per_device(): pl.pallas_call(body, out_shape=jax.ShapeDtypeStruct((own, HEADS * VDIM),...]
    all_to_all x4 -> x0, waiting for transfers between devices: 74.8 us -> none  [the longest x1 36.5 us: per_device(): lax.all_to_all(keyval, 'sp', split_axis=1, concat_axis=0, tiled=True)]
    all_gather x1 -> x0, waiting for transfers between devices: 58.7 us -> none  [per_device(): lax.all_gather(kv_weight, 'dp', axis=1, tiled=True)]
    dot_general x25 -> x0, matrix products: 47.9 us -> none  [the longest x8 18 us: attend(): jnp.einsum('hqk,khd->qhd', weights, values, preferred_element_type=jnp.fl...]
    all_to_all x4 -> x0, starting transfers between devices: 34 us -> none  [the longest x1 12 us: copy_for_each(): lax.all_to_all(jnp.broadcast_to(value[None], (length, *value.shape)), axi...]
    reduce_sum x9 -> x0, other arithmetic: 11 us -> none  [the longest x8 10.2 us: attend(): jnp.sum(raised, axis=-1, keepdims=True)]
    squeeze x8 -> x0, local copies, waits for them, and re-layouts: 7.55 us -> none  [one_sequence(): lax.map(lambda piece_rows: attend(piece_rows, keys_plain, rope_seq, value...]
    all_to_all x3 -> x0, local copies, waits for them, and re-layouts: 5.84 us -> none  [the longest x1 3.59 us: per_device(): lax.all_to_all(head_queries, 'sp', split_axis=1, concat_axis=0, tiled=True)]
  transfers between devices with their start and end apart: 5 -> 0, of which waited for: 4 -> 0; matrix products, arithmetic and copies ran while one was open for 10% -> 0% of each run, Pallas kernels for 0% -> 0%
where the time goes in v1:
time: 132 us
  Pallas kernels  114 us (86%)
  local copies, waits for them, and re-layouts  13.2 us (10%)
  other arithmetic  4.72 us (4%)
    pallas_call x1, Pallas kernels, per_device(): pl.pallas_call(body, out_shape=jax.ShapeDtypeStruct((own, HEADS * VDIM),...  114 us
    reshape x2, local copies, waits for them, and re-layouts, per_device(): kv_weight.reshape(RANK, 2, 2, 2, 128).transpose(1, 3, 2, 4, 0)  7.91 us
    unnamed x4, local copies, waits for them, and re-layouts  3.18 us

profile of v1, /device:TPU:1, one launch (start us, length us, event | category | flops | bytes accessed | tf_op | source)
XLA Modules:
  0.0 131.9 jit_solution(4105863400995859072)
XLA Ops:
  0.0 0.0 copy-start
  0.0 1.2 fusion
  1.2 0.9 multiply_cosine_fusion
  2.1 0.1 copy.16
  2.2 0.1 copy.17
  2.4 1.1 fusion.2
  3.4 0.8 concatenate.13
  4.3 0.0 copy-done
  4.3 0.9 copy.20
  5.2 0.2 fusion.4
  5.4 0.1 slice.23
  5.5 0.7 copy.21
  6.1 0.1 pad_maximum_fusion
  6.2 0.3 copy.22
  6.5 1.3 maximum_bitcast_fusion.q_in
  7.8 3.2 %reshape.102 = bf16[1024,2,2,2,128]{4,3,2,1,0:T(2,128)(2,1)S(1)} reshape(bf16[1024,1024]{1,0:T(8,128)(2,1)} %param.11) | data formatting | bytes 4194304 | tf_op jit(solution)/shard_map/reshape | solution.py:355
  11.0 4.7 %copy.23 = bf16[1024,2,2,2,128]{0,4,2,3,1:T(8,128)(2,1)} copy(bf16[1024,2,2,2,128]{4,3,2,1,0:T(2,128)(2,1)S(1)} %reshape.102) | data formatting | bytes 4194304 | tf_op jit(solution)/shard_map/reshape | solution.py:355
  15.7 113.9 %latent_attention.1 = bf16[128,4096]{1,0:T(8,128)(2,1)} custom-call(bf16[2,64,1152]{2,1,0:T(8,128)(2,1)} %bitcast.15, bf16[16,3,128,128]{3,2,1,0:T(8,128)(2,1)} %maximum_bitcast_fusion.q_in, bf16[2,512,1024]{2,1,0:T(8,128)(2,1)} %bitcast.13, bf16[128,4096]{1,0:T(8,128)(2,1)} %gate.1, f32[1,4096]{1,0:T(1,128)} %bitcast.16), custom_call_target="tpu_custom_call" | custom-call | flops 30000001024 | bytes 10000000 | tf_op jit(solution)/shard_map/latent_attention/pallas_call | solution.py:359
  129.6 2.3 %copy.25 = bf16[128,4096]{1,0:T(8,128)(2,1)} copy(bf16[128,4096]{1,0:T(8,128)(2,1)} %latent_attention.1) | data formatting | bytes 2097152
  (3 shorter events, 0.0 us)
Async XLA Ops:
  0.0 4.3 %copy-start = (bf16[128,6144]{1,0:T(8,128)(2,1)S(1)}, bf16[128,6144]{1,0:T(8,128)(2,1)}, u32[]{:S(2)}) copy-start(bf16[128,6144]{1,0:T(8,128)(2,1)} %param.7) | copy-start | bytes 4718596

commit v2 on v1

--- a/solution.py
+++ b/solution.py
@@ -20,7 +20,24 @@
 WIDE = RANK + 128
 NT = (((1,), (1,)), ((), ()))
 BF16 = jnp.bfloat16
+AWAY = (0, 1, 3, 2)
+STEP_OF = (0, 0, 1, 1, 0, 1, 2, 2, 0, 1, 2, 2, 3, 3, 3, 3, 4, 4, 4, 4)
+PLACE_OF = (0, 1, 0, 1, 2, 2, 0, 1, 3, 3, 2, 3, 0, 1, 2, 3, 0, 1, 2, 3)
+FIRST_USE = tuple(int(t not in PLACE_OF[:u]) for u, t in enumerate(PLACE_OF))
+ARRIVALS = {
+    0: ((1, 0), (1, 1)), 1: ((1, 2), (1, 3)),
+    2: ((2, 0),), 3: ((2, 1),), 4: ((2, 2),), 5: ((2, 3),),
+    7: ((3, 0),), 8: ((3, 1),), 9: ((3, 2),), 10: ((3, 3),),
+    12: ((4, 0), (4, 2)), 13: ((4, 1), (4, 3)),
+}
 F32 = jnp.float32
+
+
+def pick(table, index):
+    value = jnp.int32(table[0])
+    for i, entry in enumerate(table[1:], 1):
+        value = jnp.where(index == i, jnp.int32(entry), value)
+    return value
 
 
 def rotary(values, position):
@@ -42,7 +59,7 @@
 
 def body(
     lat_in, q_in, w_in, gate, gain, out,
-    lat, q, w, k_s, vt_s, m_s, l_s, acc_s, o_buf, o_ret, gated,
+    lat, q, qt, w, k_s, vt_s, s_s, p_s, m_s, l_s, acc_s, o_buf, o_ret, gated,
     y_send, y_recv, ring_send, ring_recv, pair_send, pair_recv,
     q_send, q_recv, w_send, w_recv, o_send, o_recv,
 ):
@@ -109,10 +126,13 @@
         def _():
             lat_copy(rr, kk).start()
 
+    def w_half(half):
+        return w_in.at[:, pl.ds(512 * half, 512)]
+
     def w_direct(half, plus):
         to = dev(xp if plus else xm, 1 - role, y, z)
         return remote(
-            w_in.at[half], w.at[2 * half + plus], w_send.at[half, plus], w_recv.at[2 * half + plus], to
+            w_half(half), w.at[2 * half + plus], w_send.at[half, plus], w_recv.at[2 * half + plus], to
         )
 
     def w_relay(half):
@@ -125,10 +145,10 @@
     @pl.when(native)
     def _():
         for half in range(2):
-            pltpu.make_async_copy(w_in.at[half], w.at[half], w_recv.at[half]).start()
-        for half in range(2):
-            for plus in range(2):
-                w_direct(half, plus).start()
+            pltpu.make_async_copy(w_half(half), w.at[half], w_recv.at[half]).start()
+        w_direct(0, 0).start()
+        w_direct(0, 1).start()
+        w_direct(1, 0).start()
 
     for t in range(4):
         for rr, kk in dests:
@@ -142,93 +162,123 @@
             def _():
                 q_copy(rr, kk, t).start()
 
-    def cut(ref, direction, step):
-        return ref.at[pl.ds(2 * direction, 2)] if step == 4 else ref
+    def source_y(i):
+        return (y + AWAY[i]) % NY
 
     def block_of(direction, step):
         return (z + NZ - step) % NZ if direction == 0 else (z + step) % NZ
 
-    def ring(direction, step):
-        block = cut(lat.at[block_of(direction, step - 1), core], direction, step)
-        return remote(
-            block, block, ring_send.at[direction, step - 1], ring_recv.at[direction, step - 1],
-            up if direction == 0 else down,
-        )
-
-    def ring_arrival(direction, step):
-        block = cut(lat.at[block_of(direction, step), core], direction, step)
-        return remote(
-            block, block, ring_send.at[direction, step - 1], ring_recv.at[direction, step - 1],
-            up if direction == 0 else down,
-        )
-
-    def to_partner(direction, step):
-        block = cut(lat.at[block_of(direction, step), core], direction, step)
-        return remote(
-            block, block, pair_send.at[direction, step], pair_recv.at[direction, step], partner
-        )
-
-    def from_partner(direction, step):
-        block = cut(lat.at[block_of(direction, step), 1 - core], direction, step)
-        return remote(
-            block, block, pair_send.at[direction, step], pair_recv.at[direction, step], partner
-        )
-
-    for yy in range(NY):
-        remote(lat_in.at[0], lat.at[z, core, yy], y_send.at[0, 0], y_recv.at[yy], partner).wait_recv()
-    ring(0, 1).start()
-    ring(1, 1).start()
-    to_partner(0, 0).start()
-
-    def advance(step):
-        for direction in range(2):
-            ring_arrival(direction, step).wait_recv()
-            if step < 4:
-                ring(direction, step + 1).start()
-            to_partner(direction, step).start()
-        for direction in range(2):
-            from_partner(direction, step).wait_recv()
+    def ring_copy(direction, step, i, have):
+        piece = lat.at[block_of(direction, step - have), core, source_y(i)]
+        at = (direction, step - 1, i)
+        return remote(piece, piece, ring_send.at[at], ring_recv.at[at], up if direction == 0 else down)
+
+    def ring(direction, step, i):
+        return ring_copy(direction, step, i, 1)
+
+    def pair_copy(direction, step, i, half):
+        piece = lat.at[block_of(direction, step), half, source_y(i)]
+        at = (direction, step, i)
+        return remote(piece, piece, pair_send.at[at], pair_recv.at[at], partner)
+
+    def carried(direction, step, i):
+        return step < 4 or i // 2 == direction
+
+    def arrive(direction, step, i):
+        ring_copy(direction, step, i, 0).wait_recv()
+        if step < 4 and carried(direction, step + 1, i):
+            ring(direction, step + 1, i).start()
+        pair_copy(direction, step, i, core).start()
+
+    def from_partner(step):
+        for direction in range(1 if step == 0 else 2):
+            for i in range(4):
+                if carried(direction, step, i):
+                    pair_copy(direction, step, i, 1 - core).wait_recv()
+
+    for i in range(4):
+        remote(
+            lat_in.at[0], lat.at[z, core, source_y(i)], y_send.at[0, 0], y_recv.at[source_y(i)], partner
+        ).wait_recv()
+        ring(0, 1, i).start()
+        ring(1, 1, i).start()
+        pair_copy(0, 0, i, core).start()
 
     def w_arrival(t):
-        return remote(w_in.at[0], w.at[t], w_send.at[0, 0], w_recv.at[t], partner)
+        return remote(w.at[0], w.at[t], w_send.at[0, 0], w_recv.at[t], partner)
 
     m_s[...] = jnp.full_like(m_s, -jnp.inf)
     l_s[...] = jnp.zeros_like(l_s)
     acc_s[...] = jnp.zeros_like(acc_s)
     lane = lax.broadcasted_iota(jnp.int32, (1, 128), 1)
 
-    def unit(t, za, zb):
-        for i, zz in enumerate((za, zb)):
-            lz = lat[zz].reshape(512, WIDE)[:, :RANK]
-            keys = lax.dot_general(lz, w[t, :256], NT, preferred_element_type=F32)
-            k_s[i * 512:(i + 1) * 512, :] = keys.astype(BF16)
-            vals = lax.dot_general(w[t, 256:], lz, NT, preferred_element_type=F32)
-            vt_s[:, i * 512:(i + 1) * 512] = vals.astype(BF16)
-        turned = jnp.concatenate(
-            [lat[zz].reshape(512, WIDE)[:, RANK:] for zz in (za, zb)], axis=0
-        )
-        for hh in range(2):
+    def unit(t, blocks):
+        n = 512 * len(blocks)
+        wk = jnp.concatenate([w[t, :, 0:128], w[t, :, 256:384]], axis=1)
+        wv = jnp.concatenate([w[t, :, 128:256], w[t, :, 384:512]], axis=1)
+        chunks = range(len(blocks))
+        rows = [slice(c * 512, (c + 1) * 512) for c in chunks]
+
+        def block(c):
+            return lat[blocks[c]].reshape(512, WIDE)
+
+        def scores(hh, c):
+            turned = block(c)[:, RANK:]
             mask = lane < 64 if hh == 0 else lane >= 64
             key = jnp.concatenate(
-                [k_s[:, hh * 128:(hh + 1) * 128], jnp.where(mask, turned, jnp.zeros_like(turned))], axis=1
+                [k_s[rows[c], hh * 128:(hh + 1) * 128], jnp.where(mask, turned, jnp.zeros_like(turned))],
+                axis=1,
             )
-            query = jnp.concatenate(
-                [
-                    jnp.concatenate([q[t, yy, hh], q[t, yy, 2]], axis=1)
-                    for yy in range(NY)
-                ],
-                axis=0,
+            s = jnp.dot(key, qt[t, hh], preferred_element_type=F32)
+            s_s[hh, rows[c], :] = s
+            top = s[0:8]
+            for g in range(1, 64):
+                top = jnp.maximum(top, s[g * 8:(g + 1) * 8])
+            return top
+
+        def peak(hh, tops):
+            top = functools.reduce(jnp.maximum, tops)
+            m_old = m_s[t, hh]
+            m_new = jnp.maximum(m_old, jnp.max(top, axis=0, keepdims=True) * SCALE)
+            m_s[t, hh] = m_new
+            return m_new, jnp.exp2(m_old - m_new)
+
+        def raise_(hh, c, m_new):
+            total = jnp.zeros((8, 512), F32)
+            low = jnp.broadcast_to(m_new, (8, 512))
+            for g in range(32):
+                row = c * 512 + g * 16
+                first = jnp.exp2(s_s[hh, row:row + 8, :] * SCALE - low)
+                second = jnp.exp2(s_s[hh, row + 8:row + 16, :] * SCALE - low)
+                total = total + (first + second)
+                p_s[hh, row:row + 16, :] = jnp.concatenate([first, second], axis=0).astype(BF16)
+            return total
+
+        def values(c):
+            v = jnp.dot(block(c)[:, :RANK], wv, preferred_element_type=F32).astype(BF16)
+            vt_s[:, rows[c]] = v.T
+
+        def finish(hh, sums, shrink):
+            l_s[t, hh] = l_s[t, hh] * shrink + jnp.sum(
+                functools.reduce(jnp.add, sums), axis=0, keepdims=True
             )
-            s = lax.dot_general(key, query, NT, preferred_element_type=F32)
-            m_old = m_s[t, hh]
-            m_new = jnp.maximum(m_old, jnp.max(s, axis=0, keepdims=True) * SCALE)
-            p = jnp.exp2(s * SCALE - m_new)
-            shrink = jnp.exp2(m_old - m_new)
-            l_s[t, hh] = l_s[t, hh] * shrink + jnp.sum(p, axis=0, keepdims=True)
-            m_s[t, hh] = m_new
             acc_s[t, hh] = acc_s[t, hh] * shrink + jnp.dot(
-                vt_s[hh * 128:(hh + 1) * 128, :], p.astype(BF16), preferred_element_type=F32
+                vt_s[hh * 128:(hh + 1) * 128, :n], p_s[hh, :n], preferred_element_type=F32
             )
+
+        for c in chunks:
+            k_s[rows[c], :] = jnp.dot(block(c)[:, :RANK], wk, preferred_element_type=F32).astype(BF16)
+        m_a, shrink_a = peak(0, [scores(0, c) for c in chunks])
+        tops, sums_a, sums_b = [], [], []
+        for c in chunks:
+            tops.append(scores(1, c))
+            sums_a.append(raise_(0, c, m_a))
+        m_b, shrink_b = peak(1, tops)
+        for c in chunks:
+            values(c)
+            sums_b.append(raise_(1, c, m_b))
+        finish(0, sums_a, shrink_a)
+        finish(1, sums_b, shrink_b)
 
     def o_copy(t, yy):
         return remote(
@@ -244,49 +294,72 @@
         w_arrival(1).wait_recv()
         w_relay(0).start()
 
-    from_partner(0, 0).wait_recv()
-
-    @pl.loop(0, 4)
-    def _(step):
-        for j in range(4):
-            @pl.when(step == j)
-            def _():
-                advance(j + 1)
-        za = jnp.where(step == 3, z, (z + NZ - 1 - step) % NZ)
-        zb = (z + 1 + step) % NZ
-
-        @pl.loop(0, 4)
-        def _(t):
-            @pl.when(step == 0)
-            def _():
-                @pl.when(jnp.logical_or(native, t != 1))
+    from_partner(0)
+
+    @pl.loop(0, len(STEP_OF))
+    def _(u):
+        step = pick(STEP_OF, u)
+        t = pick(PLACE_OF, u)
+
+        @pl.when(pick(FIRST_USE, u) == 1)
+        def _():
+            @pl.when(jnp.logical_or(native, jnp.logical_or(t == 0, t == 3)))
+            def _():
+                w_arrival(t).wait_recv()
+
+            for yy in range(NY):
+                remote(q_in.at[0], q.at[t, yy], q_send.at[0, 0, 0], q_recv.at[t, yy], partner).wait_recv()
+            for hh in range(2):
+                rows = [jnp.concatenate([q[t, yy, hh], q[t, yy, 2]], axis=1) for yy in range(NY)]
+                qt[t, hh] = jnp.concatenate(rows, axis=0).T
+
+        for j, first in ((1, 2), (2, 6), (3, 12), (4, 16)):
+            @pl.when(u == first)
+            def _():
+                from_partner(j)
+
+        single = jnp.logical_or(step == 0, step == 4)
+
+        @pl.when(single)
+        def _():
+            unit(t, [(z + step) % NZ])
+
+        @pl.when(jnp.logical_not(single))
+        def _():
+            unit(t, [(z + NZ - step) % NZ, (z + step) % NZ])
+
+        for at, what in ARRIVALS.items():
+            @pl.when(u == at)
+            def _():
+                for j, i in what:
+                    for direction in range(2):
+                        if carried(direction, j, i):
+                            arrive(direction, j, i)
+
+        @pl.when(jnp.logical_and(native, u == 1))
+        def _():
+            w_direct(1, 1).start()
+
+        @pl.when(jnp.logical_and(jnp.logical_not(native), u == 3))
+        def _():
+            w_arrival(2).wait_recv()
+            w_relay(1).start()
+
+        @pl.when(step == 4)
+        def _():
+            for hh in range(2):
+                r = acc_s[t, hh] / l_s[t, hh]
+                for yy in range(NY):
+                    piece = r[:, yy * 128:(yy + 1) * 128].T.astype(BF16)
+                    o_buf[t, yy, hh] = piece
+
+                    @pl.when(o_self(yy))
+                    def _():
+                        o_ret[pair_of(core, role, t), hh] = piece
+            for yy in range(NY):
+                @pl.when(jnp.logical_not(o_self(yy)))
                 def _():
-                    w_arrival(t).wait_recv()
-
-                @pl.when(jnp.logical_and(jnp.logical_not(native), t == 2))
-                def _():
-                    w_relay(1).start()
-
-                for yy in range(NY):
-                    remote(q_in.at[0], q.at[t, yy], q_send.at[0, 0, 0], q_recv.at[t, yy], partner).wait_recv()
-
-            unit(t, za, zb)
-
-            @pl.when(step == 3)
-            def _():
-                for hh in range(2):
-                    r = acc_s[t, hh] / l_s[t, hh]
-                    for yy in range(NY):
-                        piece = r[:, yy * 128:(yy + 1) * 128].T.astype(BF16)
-                        o_buf[t, yy, hh] = piece
-
-                        @pl.when(o_self(yy))
-                        def _():
-                            o_ret[pair_of(core, role, t), hh] = piece
-                for yy in range(NY):
-                    @pl.when(jnp.logical_not(o_self(yy)))
-                    def _():
-                        o_copy(t, yy).start()
+                    o_copy(t, yy).start()
 
     total = jnp.zeros((128, 128), F32)
     for t in range(4):
@@ -327,11 +400,13 @@
         w_relay(0).wait_send()
         w_relay(1).wait_send()
 
-    to_partner(0, 0).wait_send()
-    for direction in range(2):
-        for step in range(1, 5):
-            ring(direction, step).wait_send()
-            to_partner(direction, step).wait_send()
+    for i in range(4):
+        pair_copy(0, 0, i, core).wait_send()
+        for direction in range(2):
+            for step in range(1, 5):
+                if carried(direction, step, i):
+                    ring(direction, step, i).wait_send()
+                    pair_copy(direction, step, i, core).wait_send()
     for t in range(4):
         for yy in range(NY):
             @pl.when(jnp.logical_not(o_self(yy)))
@@ -352,7 +427,6 @@
     turned = rotary(heads[..., NOPE:], position).reshape(own, HEADS // 2, 1, 128)
     plain = heads[..., :NOPE].reshape(own, HEADS // 2, 2, 128)
     q_in = jnp.concatenate([plain, turned], axis=2).transpose(1, 2, 0, 3)
-    w_in = kv_weight.reshape(RANK, 2, 2, 2, 128).transpose(1, 3, 2, 4, 0).reshape(2, 512, RANK)
     any_spec = pl.BlockSpec(memory_space=pl.ANY)
     vmem_spec = pl.BlockSpec(memory_space=pltpu.VMEM)
     dma = pltpu.SemaphoreType.DMA
@@ -364,16 +438,19 @@
         scratch_shapes=[
             pltpu.VMEM((NZ, 2, NY, 64, WIDE), BF16),
             pltpu.VMEM((4, NY, 3, 128, 128), BF16),
-            pltpu.VMEM((4, 512, RANK), BF16),
+            pltpu.VMEM((4, 2, 256, 512), BF16),
+            pltpu.VMEM((4, RANK, 512), BF16),
             pltpu.VMEM((1024, 256), BF16),
             pltpu.VMEM((256, 1024), BF16),
+            pltpu.VMEM((2, 1024, 512), F32),
+            pltpu.VMEM((2, 1024, 512), BF16),
             pltpu.VMEM((4, 2, 1, 512), F32),
             pltpu.VMEM((4, 2, 1, 512), F32),
             pltpu.VMEM((4, 2, 128, 512), F32),
             pltpu.VMEM((4, NY, 2, 128, 128), BF16),
             pltpu.VMEM((16, 2, 128, 128), BF16),
             pltpu.VMEM((own, HEADS * VDIM), F32),
-            dma((2, 2)), dma((NY,)), dma((2, 4)), dma((2, 4)), dma((2, 5)), dma((2, 5)),
+            dma((2, 2)), dma((NY,)), dma((2, 4, 4)), dma((2, 4, 4)), dma((2, 5, 4)), dma((2, 5, 4)),
             dma((4, 2, 2)), dma((4, NY)), dma((2, 2)), dma((4,)), dma((4, NY)), dma((16,)),
         ],
         compiler_params=pltpu.CompilerParams(
@@ -381,7 +458,7 @@
         ),
         cost_estimate=pl.CostEstimate(flops=30 * 10**9, bytes_accessed=10**7, transcendentals=0),
         name="latent_attention",
-    )(lat_in, q_in, w_in, gate, out_gain.reshape(1, -1))
+    )(lat_in, q_in, kv_weight, gate, out_gain.reshape(1, -1))
 
 
 def solution(mesh):

time: 132 us -> 111 us (0.84)
  Pallas kernels: 114 us -> 101 us
  local copies, waits for them, and re-layouts: 13.2 us -> 6.31 us
  other arithmetic: 4.72 us -> 2.69 us
    pallas_call x1, Pallas kernels: 114 us -> 101 us  [per_device(): pl.pallas_call(body, out_shape=jax.ShapeDtypeStruct((own, HEADS * VDIM),...]
    reshape x2 -> x0, local copies, waits for them, and re-layouts: 7.91 us -> none  [per_device(): kv_weight.reshape(RANK, 2, 2, 2, 128).transpose(1, 3, 2, 4, 0)]
    unnamed x4 -> x6, local copies, waits for them, and re-layouts: 3.18 us -> 4.21 us
where the time goes in v2:
time: 111 us; the launch traced here: 110 us
  Pallas kernels  101 us (91%)
  local copies, waits for them, and re-layouts  6.31 us (6%)
  other arithmetic  2.69 us (2%)
    pallas_call x1, Pallas kernels, per_device(): pl.pallas_call(body, out_shape=jax.ShapeDtypeStruct((own, HEADS * VDIM),...  101 us
    unnamed x6, local copies, waits for them, and re-layouts  4.21 us

profile of v2, /device:TPU:1, one launch (start us, length us, event | category | flops | bytes accessed | tf_op | source)
XLA Modules:
  0.0 110.3 jit_solution(18049277024217040876)
XLA Ops:
  0.0 0.9 multiply_cosine_fusion
  0.9 1.9 %copy.19 = bf16[128,6144]{0,1:T(8,128)(2,1)S(1)} copy(bf16[128,6144]{1,0:T(8,128)(2,1)} %param.7) | data formatting | bytes 3145728 | tf_op args[0]
  2.8 0.2 fusion.4
  3.0 0.1 pad_maximum_fusion
  3.1 0.3 copy.21
  3.3 0.1 slice.23
  3.4 0.7 copy.20
  4.1 0.0 copy-start
  4.1 0.0 copy-start.1
  4.1 1.3 %maximum_bitcast_fusion.q_in = bf16[16,3,128,128]{3,2,1,0:T(8,128)(2,1)} fusion(bf16[128,16,1,128]{3,0,2,1:T(8,128)(2,1)S(1)} %copy.21, bf16[128,16,2,128]{3,0,2,1:T(8,128)(2,1)S(1)} %bitcast.9), kind=kLoop, calls=%fused_computation | loop fusion | flops 786432 | bytes 3145728 | tf_op jit(solution)/shard_map/transpose | solution.py:429
  5.4 0.1 copy.15
  5.6 0.1 copy.16
  5.7 0.0 copy-done
  5.7 0.1 fusion
  5.8 0.0 copy-done.1
  5.8 0.1 fusion.2
  6.0 0.8 concatenate.13
  6.8 101.2 %latent_attention.1 = bf16[128,4096]{1,0:T(8,128)(2,1)} custom-call(bf16[2,64,1152]{2,1,0:T(8,128)(2,1)} %bitcast.11, bf16[16,3,128,128]{3,2,1,0:T(8,128)(2,1)} %maximum_bitcast_fusion.q_in, bf16[1024,1024]{1,0:T(8,128)(2,1)} %w_in.1, bf16[128,4096]{1,0:T(8,128)(2,1)} %gate.1, f32[1,4096]{1,0:T(1,128)} %bitcast.12), custom_call_target="tpu_custom_call" | custom-call | flops 30000001024 | bytes 10000000 | tf_op jit(solution)/shard_map/latent_attention/pallas_call | solution.py:433
  108.0 2.3 %copy.23 = bf16[128,4096]{1,0:T(8,128)(2,1)} copy(bf16[128,4096]{1,0:T(8,128)(2,1)} %latent_attention.1) | data formatting | bytes 2097152
  (3 shorter events, 0.0 us)
Async XLA Ops:
  4.1 1.6 %copy-start = (bf16[128,1024]{1,0:T(8,128)(2,1)S(1)}, bf16[128,1024]{1,0:T(8,128)(2,1)}, u32[]{:S(2)}) copy-start(bf16[128,1024]{1,0:T(8,128)(2,1)} %param.8) | copy-start | bytes 786436
  4.1 1.7 %copy-start.1 = (f32[1024]{0:T(1024)S(1)}, f32[1024]{0:T(1024)}, u32[]{:S(2)}) copy-start(f32[1024]{0:T(1024)} %param.10) | copy-start | bytes 12292

commit v3 on v2

--- a/solution.py
+++ b/solution.py
@@ -21,8 +21,8 @@
 NT = (((1,), (1,)), ((), ()))
 BF16 = jnp.bfloat16
 AWAY = (0, 1, 3, 2)
-STEP_OF = (0, 0, 1, 1, 0, 1, 2, 2, 0, 1, 2, 2, 3, 3, 3, 3, 4, 4, 4, 4)
-PLACE_OF = (0, 1, 0, 1, 2, 2, 0, 1, 3, 3, 2, 3, 0, 1, 2, 3, 0, 1, 2, 3)
+STEP_OF = (0, 0, 1, 1, 0, 1, 2, 2, 2, 0, 1, 2, 3, 3, 3, 3, 4, 4, 4, 4)
+PLACE_OF = (0, 1, 0, 1, 2, 2, 0, 1, 2, 3, 3, 3, 0, 1, 2, 3, 0, 1, 2, 3)
 FIRST_USE = tuple(int(t not in PLACE_OF[:u]) for u, t in enumerate(PLACE_OF))
 ARRIVALS = {
     0: ((1, 0), (1, 1)), 1: ((1, 2), (1, 3)),
@@ -40,26 +40,9 @@
     return value
 
 
-def rotary(values, position):
-    half_width = values.shape[-1] // 2
-    inverse = THETA ** (-jnp.arange(half_width, dtype=F32) / half_width)
-    angles = position.astype(F32)[:, None] * inverse[None, :]
-    if values.ndim == 3:
-        angles = angles[:, None, :]
-    cosine = jnp.cos(angles)
-    sine_part = jnp.sin(angles)
-    front_half = values[..., :half_width].astype(F32)
-    back_half = values[..., half_width:].astype(F32)
-    turned = jnp.concatenate(
-        [front_half * cosine - back_half * sine_part, back_half * cosine + front_half * sine_part],
-        axis=-1,
-    )
-    return turned.astype(BF16)
-
-
 def body(
-    lat_in, q_in, w_in, gate, gain, out,
-    lat, q, qt, w, k_s, vt_s, s_s, p_s, m_s, l_s, acc_s, o_buf, o_ret, gated,
+    queries, latent, rope_key, latent_gain, cosine, sine, w_in, gate, gain, out,
+    lat_in, q_in, lat, q, qt, w, k_s, vt_s, s_s, p_s, m_s, l_s, acc_s, o_buf, o_ret, gated,
     y_send, y_recv, ring_send, ring_recv, pair_send, pair_recv,
     q_send, q_recv, w_send, w_recv, o_send, o_recv,
 ):
@@ -98,6 +81,28 @@
                 pl.semaphore_signal(barrier, inc=1, device_id=dev(x, cc, yy, z), device_id_type=pl.DeviceIdType.MESH)
     for to in (up, down, dev(xp, 0, y, z), dev(xp, 1, y, z), dev(xm, 0, y, z), dev(xm, 1, y, z)):
         pl.semaphore_signal(barrier, inc=1, device_id=to, device_id_type=pl.DeviceIdType.MESH)
+
+    @pl.when(native)
+    def _():
+        for half in range(2):
+            pltpu.make_async_copy(w_in.at[:, pl.ds(512 * half, 512)], w.at[half], w_recv.at[half]).start()
+
+    lane = lax.broadcasted_iota(jnp.int32, (1, 128), 1)
+
+    def rotated(pair):
+        other = jnp.where(lane % 64 < 32, pltpu.roll(pair, 96, 1), pltpu.roll(pair, 32, 1))
+        return (pair * cosine[...] + other * sine[...]).astype(BF16)
+
+    wide = latent[...].astype(F32)
+    level = lax.rsqrt(jnp.mean(wide * wide, axis=1, keepdims=True) + EPS)
+    normed = (wide * level * latent_gain[...]).astype(BF16)
+    key = rope_key[...].astype(F32)
+    turned_key = rotated(jnp.concatenate([key, key], axis=1))
+    for half in range(2):
+        rows = slice(half * 64, (half + 1) * 64)
+        lat_in[half, :, :RANK] = normed[rows]
+        lat_in[half, :, RANK:] = turned_key[rows]
+
     pl.semaphore_wait(barrier, 13)
 
     dests = [(rr, kk) for rr in range(2) for kk in range(2)]
@@ -116,15 +121,6 @@
             q_in.at[pair_of(kk, rr, t)], q.at[t, y], q_send.at[t, rr, kk], q_recv.at[t, y],
             dev(x, kk, 2 * core + rr, z),
         )
-
-    for rr, kk in dests:
-        @pl.when(is_self(rr, kk))
-        def _():
-            pltpu.make_async_copy(lat_in.at[kk], lat.at[z, kk, y], y_recv.at[y]).start()
-
-        @pl.when(jnp.logical_not(is_self(rr, kk)))
-        def _():
-            lat_copy(rr, kk).start()
 
     def w_half(half):
         return w_in.at[:, pl.ds(512 * half, 512)]
@@ -144,23 +140,39 @@
 
     @pl.when(native)
     def _():
-        for half in range(2):
-            pltpu.make_async_copy(w_half(half), w.at[half], w_recv.at[half]).start()
         w_direct(0, 0).start()
         w_direct(0, 1).start()
         w_direct(1, 0).start()
 
+    for rr, kk in dests:
+        @pl.when(is_self(rr, kk))
+        def _():
+            lat[z, kk, y] = lat_in[kk]
+
+        @pl.when(jnp.logical_not(is_self(rr, kk)))
+        def _():
+            lat_copy(rr, kk).start()
+
+    for g in range(HEADS // 2):
+        plain = queries[:, g * 384:g * 384 + 128]
+        left = queries[:, g * 384 + 128:g * 384 + 256].astype(F32)
+        right = queries[:, g * 384 + 256:g * 384 + 384].astype(F32)
+        q_in[g, 0] = plain
+        q_in[g, 1] = pltpu.roll(jnp.where(lane < 64, right, left), 64, 1).astype(BF16)
+        q_in[g, 2] = rotated(jnp.where(lane < 64, left, right))
+
     for t in range(4):
         for rr, kk in dests:
             @pl.when(is_self(rr, kk))
             def _():
-                pltpu.make_async_copy(
-                    q_in.at[pair_of(kk, rr, t)], q.at[t, y], q_recv.at[t, y]
-                ).start()
+                q[t, y] = q_in[pair_of(kk, rr, t)]
 
             @pl.when(jnp.logical_not(is_self(rr, kk)))
             def _():
                 q_copy(rr, kk, t).start()
+
+    def own_seq(yy):
+        return jnp.logical_and(seq == core, yy == y)
 
     def source_y(i):
         return (y + AWAY[i]) % NY
@@ -197,9 +209,12 @@
                     pair_copy(direction, step, i, 1 - core).wait_recv()
 
     for i in range(4):
-        remote(
-            lat_in.at[0], lat.at[z, core, source_y(i)], y_send.at[0, 0], y_recv.at[source_y(i)], partner
-        ).wait_recv()
+        @pl.when(jnp.logical_not(own_seq(source_y(i))))
+        def _():
+            remote(
+                lat_in.at[0], lat.at[z, core, source_y(i)], y_send.at[0, 0], y_recv.at[source_y(i)], partner
+            ).wait_recv()
+
         ring(0, 1, i).start()
         ring(1, 1, i).start()
         pair_copy(0, 0, i, core).start()
@@ -210,7 +225,10 @@
     m_s[...] = jnp.full_like(m_s, -jnp.inf)
     l_s[...] = jnp.zeros_like(l_s)
     acc_s[...] = jnp.zeros_like(acc_s)
-    lane = lax.broadcasted_iota(jnp.int32, (1, 128), 1)
+    for h in range(HEADS):
+        cols = slice(h * 128, (h + 1) * 128)
+        v = gate[:, cols].astype(F32)
+        gated[:, cols] = v / (1.0 + jnp.exp(-v))
 
     def unit(t, blocks):
         n = 512 * len(blocks)
@@ -308,7 +326,11 @@
                 w_arrival(t).wait_recv()
 
             for yy in range(NY):
-                remote(q_in.at[0], q.at[t, yy], q_send.at[0, 0, 0], q_recv.at[t, yy], partner).wait_recv()
+                @pl.when(jnp.logical_not(own_seq(yy)))
+                def _():
+                    remote(
+                        q_in.at[0], q.at[t, yy], q_send.at[0, 0, 0], q_recv.at[t, yy], partner
+                    ).wait_recv()
             for hh in range(2):
                 rows = [jnp.concatenate([q[t, yy, hh], q[t, yy, 2]], axis=1) for yy in range(NY)]
                 qt[t, hh] = jnp.concatenate(rows, axis=0).T
@@ -336,7 +358,7 @@
                         if carried(direction, j, i):
                             arrive(direction, j, i)
 
-        @pl.when(jnp.logical_and(native, u == 1))
+        @pl.when(jnp.logical_and(native, u == 3))
         def _():
             w_direct(1, 1).start()
 
@@ -371,11 +393,12 @@
                 remote(
                     o_buf.at[0, 0], o_ret.at[g], o_send.at[0, 0], o_recv.at[g], partner
                 ).wait_recv()
-    for h in range(HEADS):
-        v = gate[:, h * 128:(h + 1) * 128].astype(F32)
-        piece = o_ret[h // 2, h % 2].astype(F32) * (v / (1.0 + jnp.exp(-v)))
-        gated[:, h * 128:(h + 1) * 128] = piece
-        total = total + piece * piece
+
+            for hh in range(2):
+                cols = pl.ds(pl.multiple_of(g * 256 + hh * 128, 128), 128)
+                piece = o_ret[g, hh].astype(F32) * gated[:, cols]
+                gated[:, cols] = piece
+                total = total + piece * piece
     mean = jnp.sum(total, axis=1, keepdims=True) / (HEADS * VDIM)
     scale = lax.rsqrt(mean + EPS)
     for h in range(HEADS):
@@ -417,25 +440,21 @@
 def per_device(queries, latent, rope_key, latent_gain, kv_weight, gate, out_gain):
     own = queries.shape[0]
     position = lax.axis_index("sp") * own + jnp.arange(own, dtype=jnp.int32)
-    widened = latent.astype(F32)
-    normed = (
-        widened * lax.rsqrt(jnp.mean(widened * widened, axis=-1, keepdims=True) + EPS) * latent_gain
-    ).astype(BF16)
-    turned_key = rotary(rope_key, position)
-    lat_in = jnp.concatenate([normed, turned_key, turned_key], axis=1).reshape(2, 64, WIDE)
-    heads = queries.reshape(own, HEADS, NOPE + ROPE)
-    turned = rotary(heads[..., NOPE:], position).reshape(own, HEADS // 2, 1, 128)
-    plain = heads[..., :NOPE].reshape(own, HEADS // 2, 2, 128)
-    q_in = jnp.concatenate([plain, turned], axis=2).transpose(1, 2, 0, 3)
+    half = jnp.arange(ROPE // 2, dtype=F32)
+    angles = position.astype(F32)[:, None] * jnp.tile(THETA ** (-half / (ROPE // 2)), 4)[None, :]
+    sign = jnp.where(jnp.arange(128) % ROPE < ROPE // 2, -1.0, 1.0)
+    cosine, sine = jnp.cos(angles), jnp.sin(angles) * sign[None, :]
     any_spec = pl.BlockSpec(memory_space=pl.ANY)
     vmem_spec = pl.BlockSpec(memory_space=pltpu.VMEM)
     dma = pltpu.SemaphoreType.DMA
     return pl.pallas_call(
         body,
         out_shape=jax.ShapeDtypeStruct((own, HEADS * VDIM), BF16),
-        in_specs=[any_spec, any_spec, any_spec, vmem_spec, vmem_spec],
+        in_specs=[vmem_spec] * 6 + [any_spec, vmem_spec, vmem_spec],
         out_specs=vmem_spec,
         scratch_shapes=[
+            pltpu.VMEM((2, own // 2, WIDE), BF16),
+            pltpu.VMEM((HEADS // 2, 3, 128, 128), BF16),
             pltpu.VMEM((NZ, 2, NY, 64, WIDE), BF16),
             pltpu.VMEM((4, NY, 3, 128, 128), BF16),
             pltpu.VMEM((4, 2, 256, 512), BF16),
@@ -458,7 +477,10 @@
         ),
         cost_estimate=pl.CostEstimate(flops=30 * 10**9, bytes_accessed=10**7, transcendentals=0),
         name="latent_attention",
-    )(lat_in, q_in, kv_weight, gate, out_gain.reshape(1, -1))
+    )(
+        queries, latent, rope_key, latent_gain.reshape(1, -1), cosine, sine,
+        kv_weight, gate, out_gain.reshape(1, -1),
+    )
 
 
 def solution(mesh):

time: 111 us -> 99.1 us (0.89)
  Pallas kernels: 101 us -> 94.1 us
  local copies, waits for them, and re-layouts: 6.31 us -> 3.8 us
  other arithmetic: 2.69 us -> 0.98 us
    pallas_call x1, Pallas kernels: 101 us -> 94.1 us  [per_device(): pl.pallas_call(body, out_shape=jax.ShapeDtypeStruct((own, HEADS * VDIM),...]
    transpose x1 -> x0, other arithmetic: 1.3 us -> none  [per_device(): q_in = jnp.concatenate([plain, turned], axis=2).transpose(1, 2, 0, 3)]
    unnamed x6 -> x2, local copies, waits for them, and re-layouts: 4.21 us -> 3.72 us
where the time goes in v3:
time: 99.1 us; the launch traced here: 98.9 us
  Pallas kernels  94.1 us (95%)
  local copies, waits for them, and re-layouts  3.8 us (4%)
    pallas_call x1, Pallas kernels, per_device(): pl.pallas_call(body, out_shape=jax.ShapeDtypeStruct((own, HEADS * VDIM),...  94.1 us
    unnamed x2, local copies, waits for them, and re-layouts  3.72 us

profile of v3, /device:TPU:1, one launch (start us, length us, event | category | flops | bytes accessed | tf_op | source)
XLA Modules:
  0.0 98.9 jit_solution(9788172794718866568)
XLA Ops:
  0.0 0.1 mul.28
  0.1 1.4 %copy.8.rope_key = bf16[128,64]{1,0:T(8,128)(2,1)} copy(bf16[128,64]{0,1:T(8,128)(2,1)} %param.9) | data formatting | bytes 32768 | tf_op args[2]
  1.5 1.0 fusion
  2.5 94.1 %latent_attention.1 = bf16[128,4096]{1,0:T(8,128)(2,1)} custom-call(bf16[128,6144]{1,0:T(8,128)(2,1)} %queries.1, bf16[128,1024]{1,0:T(8,128)(2,1)} %latent.1, bf16[128,64]{1,0:T(8,128)(2,1)} %copy.8.rope_key, f32[1,1024]{1,0:T(1,128)} %bitcast.3, f32[128,128]{1,0:T(8,128)} %get-tuple-element.6.cosine, f32[128,128]{1,0:T(8,128)} %get-tuple-element.5.sine, ...), custom_call_target="tpu_custom_call" | custom-call | flops 30000001024 | bytes 10000000 | tf_op jit(solution)/shard_map/latent_attention/pallas_call | solution.py:450
  96.6 2.3 %copy.10 = bf16[128,4096]{1,0:T(8,128)(2,1)} copy(bf16[128,4096]{1,0:T(8,128)(2,1)} %latent_attention.1) | data formatting | bytes 2097152
  (4 shorter events, 0.0 us)

commit v4 on v3

--- a/solution.py
+++ b/solution.py
@@ -21,14 +21,14 @@
 NT = (((1,), (1,)), ((), ()))
 BF16 = jnp.bfloat16
 AWAY = (0, 1, 3, 2)
-STEP_OF = (0, 0, 1, 1, 0, 1, 2, 2, 2, 0, 1, 2, 3, 3, 3, 3, 4, 4, 4, 4)
-PLACE_OF = (0, 1, 0, 1, 2, 2, 0, 1, 2, 3, 3, 3, 0, 1, 2, 3, 0, 1, 2, 3)
+STEP_OF = (0, 0, 1, 1, 0, 1, 2, 2, 2, 0, 1, 2, 3, 3, 3, 3, 4, 4, 4, 4, 5, 5, 5, 5)
+PLACE_OF = (0, 1, 0, 1, 2, 2, 0, 1, 2, 3, 3, 3, 0, 1, 2, 3, 0, 1, 2, 3, 0, 1, 2, 3)
 FIRST_USE = tuple(int(t not in PLACE_OF[:u]) for u, t in enumerate(PLACE_OF))
 ARRIVALS = {
     0: ((1, 0), (1, 1)), 1: ((1, 2), (1, 3)),
     2: ((2, 0),), 3: ((2, 1),), 4: ((2, 2),), 5: ((2, 3),),
-    7: ((3, 0),), 8: ((3, 1),), 9: ((3, 2),), 10: ((3, 3),),
-    12: ((4, 0), (4, 2)), 13: ((4, 1), (4, 3)),
+    7: ((3, 0),), 8: ((3, 1),), 12: ((3, 2),), 13: ((3, 3),),
+    16: ((4, 0), (4, 2)), 17: ((4, 1), (4, 3)),
 }
 F32 = jnp.float32
 
@@ -202,9 +202,9 @@
             ring(direction, step + 1, i).start()
         pair_copy(direction, step, i, core).start()
 
-    def from_partner(step):
+    def from_partner(step, pieces=(0, 1, 2, 3)):
         for direction in range(1 if step == 0 else 2):
-            for i in range(4):
+            for i in pieces:
                 if carried(direction, step, i):
                     pair_copy(direction, step, i, 1 - core).wait_recv()
 
@@ -238,7 +238,7 @@
         rows = [slice(c * 512, (c + 1) * 512) for c in chunks]
 
         def block(c):
-            return lat[blocks[c]].reshape(512, WIDE)
+            return blocks[c]()
 
         def scores(hh, c):
             turned = block(c)[:, RANK:]
@@ -335,20 +335,37 @@
                 rows = [jnp.concatenate([q[t, yy, hh], q[t, yy, 2]], axis=1) for yy in range(NY)]
                 qt[t, hh] = jnp.concatenate(rows, axis=0).T
 
-        for j, first in ((1, 2), (2, 6), (3, 12), (4, 16)):
+        for j, first, pieces in (
+            (1, 2, range(4)), (2, 6, range(4)), (3, 12, (0, 1)), (3, 16, (2, 3)), (4, 20, range(4))
+        ):
             @pl.when(u == first)
             def _():
-                from_partner(j)
-
-        single = jnp.logical_or(step == 0, step == 4)
+                from_partner(j, pieces)
+
+        single = jnp.logical_or(step == 0, step >= 3)
+        mixed = jnp.logical_or(step == 3, step == 4)
+
+        def whole(zz):
+            return lambda: lat[zz].reshape(512, WIDE)
+
+        def parts():
+            rows = []
+            for k in range(4):
+                alone = jnp.where(step == 5, (z + 4) % NZ, z)
+                zz = jnp.where(mixed, block_of(k // 2, 3), alone)
+                away = jnp.where(step == 4, AWAY[k % 2 + 2], AWAY[k % 2])
+                yy = (y + jnp.where(mixed, away, AWAY[k])) % NY
+                rows += [lat[zz, 0, yy], lat[zz, 1, yy]]
+            return jnp.concatenate(rows, axis=0)
+
 
         @pl.when(single)
         def _():
-            unit(t, [(z + step) % NZ])
+            unit(t, [parts])
 
         @pl.when(jnp.logical_not(single))
         def _():
-            unit(t, [(z + NZ - step) % NZ, (z + step) % NZ])
+            unit(t, [whole((z + NZ - step) % NZ), whole((z + step) % NZ)])
 
         for at, what in ARRIVALS.items():
             @pl.when(u == at)
@@ -367,7 +384,7 @@
             w_arrival(2).wait_recv()
             w_relay(1).start()
 
-        @pl.when(step == 4)
+        @pl.when(step == 5)
         def _():
             for hh in range(2):
                 r = acc_s[t, hh] / l_s[t, hh]

time: 99.1 us -> 104 us (1.049)
  Pallas kernels: 94.1 us -> 98.9 us
    pallas_call x1, Pallas kernels: 94.1 us -> 98.9 us  [per_device(): pl.pallas_call(body, out_shape=jax.ShapeDtypeStruct((own, HEADS * VDIM),...]
where the time goes in v4:
time: 104 us
  Pallas kernels  98.9 us (95%)
  local copies, waits for them, and re-layouts  3.8 us (4%)
    pallas_call x1, Pallas kernels, per_device(): pl.pallas_call(body, out_shape=jax.ShapeDtypeStruct((own, HEADS * VDIM),...  98.9 us
    unnamed x2, local copies, waits for them, and re-layouts  3.72 us

profile of v4, /device:TPU:1, one launch (start us, length us, event | category | flops | bytes accessed | tf_op | source)
XLA Modules:
  0.0 103.7 jit_solution(8169808660502726899)
XLA Ops:
  0.0 0.1 mul.28
  0.1 1.4 %copy.8.rope_key = bf16[128,64]{1,0:T(8,128)(2,1)} copy(bf16[128,64]{0,1:T(8,128)(2,1)} %param.9) | data formatting | bytes 32768 | tf_op args[2]
  1.5 1.0 fusion
  2.5 98.9 %latent_attention.1 = bf16[128,4096]{1,0:T(8,128)(2,1)} custom-call(bf16[128,6144]{1,0:T(8,128)(2,1)} %queries.1, bf16[128,1024]{1,0:T(8,128)(2,1)} %latent.1, bf16[128,64]{1,0:T(8,128)(2,1)} %copy.8.rope_key, f32[1,1024]{1,0:T(1,128)} %bitcast.3, f32[128,128]{1,0:T(8,128)} %get-tuple-element.6.cosine, f32[128,128]{1,0:T(8,128)} %get-tuple-element.5.sine, ...), custom_call_target="tpu_custom_call" | custom-call | flops 30000001024 | bytes 10000000 | tf_op jit(solution)/shard_map/latent_attention/pallas_call | solution.py:467
  101.4 2.3 %copy.10 = bf16[128,4096]{1,0:T(8,128)(2,1)} copy(bf16[128,4096]{1,0:T(8,128)(2,1)} %latent_attention.1) | data formatting | bytes 2097152
  (4 shorter events, 0.0 us)
